TPU v7x, 32 devices: a whole 2x2x4 slice. The times are simulated.
32 devices in a mesh: fs: 8 (over z, y), tp: 4 (over x, core).
Axes of the slice: x: 2, y: 2, z: 4, core: 2. Of those that a mesh axis runs over, the one named last changes fastest.
Arguments:
- tokens: bfloat16 [8192, 2048], P('fs', 'tp'), may hold values from -6 to 6
- mixer_gain: float32 [2048], replicated, may hold values from 0.1 to 1.9
- conv_taps: bfloat16 [3, 1024], replicated, may hold values from -3.5 to 3.5
- outer_weight: bfloat16 [2048, 1024], P('fs', 'tp'), may hold values from -0.125 to 0.125
- inner_weight: bfloat16 [2048, 1024], P('fs', 'tp'), may hold values from -0.125 to 0.125
- value_weight: bfloat16 [2048, 1024], P('fs', 'tp'), may hold values from -0.125 to 0.125
- merge_weight: bfloat16 [1024, 2048], P('tp', 'fs'), may hold values from -0.25 to 0.25
- merge_gain: float32 [2048], replicated, may hold values from 0.1 to 1.9
- channel_gain: float32 [2048], replicated, may hold values from 0.1 to 1.9
- gate_weight: bfloat16 [2048, 5632], P('fs', 'tp'), may hold values from -0.125 to 0.125
- up_weight: bfloat16 [2048, 5632], P('fs', 'tp'), may hold values from -0.125 to 0.125
- down_weight: bfloat16 [5632, 2048], P('tp', 'fs'), may hold values from -0.109375 to 0.109375
- output_gain: float32 [2048], replicated, may hold values from 0.1 to 1.9
Outputs:
- layer_out: bfloat16 [8192, 2048], P('fs', 'tp')
All inputs are finite; a program needn't handle non-finite values.
Results may differ from a plain program's by a relative error of at most 0.018.
Values may be sent and summed in bfloat16 or wider, within the bound.
A program may use at most 128 MiB of HBM per device.

v0:
```python
import jax
import jax.numpy as jnp
from jax import lax
from jax.sharding import PartitionSpec as P

HEAD_DIM = 128
EPS = 1e-06


def normalize(values):
    floats = values.astype(jnp.float32)
    return floats * lax.rsqrt(jnp.mean(floats * floats, axis=-1, keepdims=True) + EPS)


def rounded_term(partial_value):
    return lax.optimization_barrier(partial_value.astype(jnp.bfloat16)).astype(jnp.float32)


def finish_scatter(summed, residual, gain_row, squares):
    floats = summed.astype(jnp.float32)
    columns = floats.shape[1]
    factor = lax.rsqrt(squares / (columns * lax.axis_size("tp")) + EPS)
    own_gain = lax.dynamic_slice_in_dim(gain_row, lax.axis_index("tp") * columns, columns)
    return (residual.astype(jnp.float32) + floats * factor[:, None] * own_gain).astype(jnp.bfloat16)


def shards(
    tokens,
    mixer_gain,
    conv_taps,
    outer_weight,
    inner_weight,
    value_weight,
    merge_weight,
    merge_gain,
    channel_gain,
    gate_weight,
    up_weight,
    down_weight,
    output_gain,
):
    whole_tokens = lax.all_gather(tokens, "tp", axis=1, tiled=True)
    normed = (normalize(whole_tokens) * mixer_gain).astype(jnp.bfloat16)
    length = normed.shape[0]
    channels = outer_weight.shape[1]
    full_outer, full_inner, full_value = (
        lax.all_gather(outer_weight, "fs", axis=0, tiled=True),
        lax.all_gather(inner_weight, "fs", axis=0, tiled=True),
        lax.all_gather(value_weight, "fs", axis=0, tiled=True),
    )
    outer = jnp.dot(normed, full_outer, preferred_element_type=jnp.float32)
    inner = jnp.dot(normed, full_inner, preferred_element_type=jnp.float32)
    value = jnp.dot(normed, full_value, preferred_element_type=jnp.float32)
    own_taps = lax.dynamic_slice_in_dim(
        conv_taps, lax.axis_index("tp") * channels, channels, 1
    ).astype(jnp.float32)
    signal = inner * value
    padded = jnp.pad(signal, ((2, 0), (0, 0)))
    conv = (
        own_taps[0] * padded[:length]
        + own_taps[1] * padded[1 : length + 1]
        + own_taps[2] * padded[2:]
    )
    gated = (outer * conv).reshape(length, channels // HEAD_DIM, HEAD_DIM)
    mixed = normalize(gated).reshape(length, channels).astype(jnp.bfloat16)
    merged_part = jnp.dot(
        mixed,
        lax.all_gather(merge_weight, "fs", axis=1, tiled=True),
        preferred_element_type=jnp.float32,
    )
    merged = lax.psum(rounded_term(merged_part).astype(jnp.bfloat16), "tp")
    first_full = (whole_tokens.astype(jnp.float32) + normalize(merged) * merge_gain).astype(
        jnp.bfloat16
    )
    width = tokens.shape[1]
    first = lax.dynamic_slice_in_dim(first_full, lax.axis_index("tp") * width, width, 1)
    normed2 = (normalize(first_full) * channel_gain).astype(jnp.bfloat16)
    full_gate, full_up = (
        lax.all_gather(gate_weight, "fs", axis=0, tiled=True),
        lax.all_gather(up_weight, "fs", axis=0, tiled=True),
    )
    gate = jnp.dot(normed2, full_gate, preferred_element_type=jnp.float32)
    upward = jnp.dot(normed2, full_up, preferred_element_type=jnp.float32)
    hidden = (jax.nn.silu(gate) * upward).astype(jnp.bfloat16)
    down_part = jnp.dot(
        hidden,
        lax.all_gather(down_weight, "fs", axis=1, tiled=True),
        preferred_element_type=jnp.float32,
    )
    down = lax.psum_scatter(
        rounded_term(down_part).astype(jnp.bfloat16), "tp", scatter_dimension=1, tiled=True
    )
    down_float = down.astype(jnp.float32)
    down_squares = lax.psum(jnp.sum(down_float * down_float, axis=1), "tp")
    return finish_scatter(down, first, output_gain, down_squares)


def solution(mesh):
    return jax.shard_map(
        shards,
        mesh=mesh,
        in_specs=(
            P("fs", "tp"),
            P(),
            P(),
            P("fs", "tp"),
            P("fs", "tp"),
            P("fs", "tp"),
            P("tp", "fs"),
            P(),
            P(),
            P("fs", "tp"),
            P("fs", "tp"),
            P("tp", "fs"),
            P(),
        ),
        out_specs=P("fs", "tp"),
        check_vma=False,
    )
```

profile of v0, /device:TPU:0, one launch (start us, length us, event | category | flops | bytes accessed | tf_op | source)
XLA Modules:
  0.0 661.4 jit_solution(1043669761443059637)
XLA Ops:
  6.5 0.7 all-gather.9.cloned.1.call-update
  10.7 35.5 %all-gather.9.cloned.1.call-done = bf16[1024,2048]{1,0:T(8,128)(2,1)} async-done(((bf16[1024,512]{1,0:T(8,128)(2,1)}), bf16[1024,2048]{1,0:T(8,128)(2,1)}) %all-gather.9.cloned.1.call-update) | async-done | bytes 4194320 | tf_op jit(solution)/shard_map/all_gather | solution.py:42
  46.1 3.1 fusion.5
  49.2 39.4 %all-gather.13.cloned.1.call-done = bf16[2048,256]{1,0:T(8,128)(2,1)} async-done(((bf16[256,256]{1,0:T(8,128)(2,1)}), bf16[2048,256]{1,0:T(8,128)(2,1)}) %all-gather.13.cloned.1.call-update) | async-done | bytes 1048592 | tf_op jit(solution)/shard_map/all_gather | solution.py:48
  88.5 4.0 fusion.22
  92.5 37.2 %all-gather.15.cloned.1.call-done = bf16[2048,256]{1,0:T(8,128)(2,1)} async-done(((bf16[256,256]{1,0:T(8,128)(2,1)}), bf16[2048,256]{1,0:T(8,128)(2,1)}) %all-gather.15.cloned.1.call-update) | async-done | bytes 1048592 | tf_op jit(solution)/shard_map/all_gather | solution.py:49
  129.7 4.0 convolution_multiply_fusion
  133.7 37.0 %all-gather.11.cloned.1.call-done = bf16[2048,256]{1,0:T(8,128)(2,1)} async-done(((bf16[256,256]{1,0:T(8,128)(2,1)}), bf16[2048,256]{1,0:T(8,128)(2,1)}) %all-gather.11.cloned.1.call-update) | async-done | bytes 1048592 | tf_op jit(solution)/shard_map/all_gather | solution.py:47
  170.7 4.4 bitcast_reduce_fusion
  175.2 35.5 %all-gather.17.cloned.1.call-done = bf16[256,2048]{1,0:T(8,128)(2,1)} async-done(((bf16[256,256]{1,0:T(8,128)(2,1)}), bf16[256,2048]{1,0:T(8,128)(2,1)}) %all-gather.17.cloned.1.call-update) | async-done | bytes 1048592 | tf_op jit(solution)/shard_map/all_gather | solution.py:68
  210.7 4.6 convolution_convert_fusion.1
  217.8 82.2 %all-reduce.3.cloned.1.call-done = bf16[1024,2048]{1,0:T(8,128)(2,1)} async-done(((bf16[1024,2048]{1,0:T(8,128)(2,1)}), bf16[1024,2048]{1,0:T(8,128)(2,1)}) %all-reduce.3.cloned.1.call-update) | async-done | bytes 4194320 | tf_op jit(solution)/shard_map/psum | solution.py:71
  300.0 3.2 fusion
  303.4 5.3 fusion.2
  308.8 85.9 %all-gather.19.cloned.1.call-done = bf16[2048,1408]{1,0:T(8,128)(2,1)} async-done(((bf16[256,1408]{1,0:T(8,128)(2,1)}), bf16[2048,1408]{1,0:T(8,128)(2,1)}) %all-gather.19.cloned.1.call-update) | async-done | bytes 5767184 | tf_op jit(solution)/shard_map/all_gather | solution.py:79
  394.6 12.0 %fusion.14 = f32[1024,1408]{1,0:T(8,128)} fusion(bf16[2048,1408]{1,0:T(8,128)(2,1)} %all-gather.19.cloned.1.call-done, bf16[1024,2048]{1,0:T(8,128)(2,1)} %get-tuple-element.6, f32[2048]{0:T(1024)S(1)} %copy-done.3, f32[1024]{0:T(1024)S(1)} %add_rsqrt_fusion.2), kind=kOutput, calls=%fused_computation.27 | convolution fusion | flops 5913968640 | bytes 15740928 | tf_op jit(solution)/shard_map/dot_general | solution.py:82
  406.6 80.7 %all-gather.21.cloned.1.call-done = bf16[2048,1408]{1,0:T(8,128)(2,1)} async-done(((bf16[256,1408]{1,0:T(8,128)(2,1)}), bf16[2048,1408]{1,0:T(8,128)(2,1)}) %all-gather.21.cloned.1.call-update) | async-done | bytes 5767184 | tf_op jit(solution)/shard_map/all_gather | solution.py:80
  487.3 93.4 %all-gather.23.cloned.1.call-done = bf16[1408,2048]{1,0:T(8,128)(2,1)} async-done(((bf16[1408,256]{1,0:T(8,128)(2,1)}), bf16[1408,2048]{1,0:T(8,128)(2,1)}) %all-gather.23.cloned.1.call-update) | async-done | bytes 5767184 | tf_op jit(solution)/shard_map/all_gather | solution.py:87
  580.7 20.8 %convolution_convert_fusion = bf16[1024,2048]{1,0:T(8,128)(2,1)} fusion(bf16[1408,2048]{1,0:T(8,128)(2,1)} %all-gather.23.cloned.1.call-done, f32[1024,1408]{1,0:T(8,128)} %fusion.14, bf16[2048,1408]{1,0:T(8,128)(2,1)} %all-gather.21.cloned.1.call-done, bf16[1024,2048]{1,0:T(8,128)(2,1)} %get-tuple-element.6, f32[2048]{0:T(1024)S(1)} %copy-done.3, ...), kind=kOutput, calls=%fused_computation.17 | convolution fusion | flops 11830296576 | bytes 25702400 | tf_op jit(solution)/shard_map/dot_general | solution.py:85
  601.6 0.8 dynamic_slice.11
  602.3 42.0 %reduce-scatter.2.cloned.1.call-done = bf16[1024,512]{1,0:T(8,128)(2,1)} async-done(((bf16[1024,2048]{1,0:T(8,128)(2,1)}), bf16[1024,512]{1,0:T(8,128)(2,1)}) %reduce-scatter.2.cloned.1.call-update) | async-done | bytes 1048592 | tf_op jit(solution)/shard_map/reduce_scatter | solution.py:90
  644.3 1.5 fusion.9
  645.8 5.8 psum.15
  651.6 3.0 fusion.12
  (35 shorter events, 6.1 us)
Async XLA Ops:
  6.5 82.0 %copy-start.2 = (f32[2048]{0:T(1024)S(1)}, f32[2048]{0:T(1024)}, u32[]{:S(2)}) copy-start(f32[2048]{0:T(1024)} %param.14) | copy-start | bytes 24580
  6.5 39.6 %all-gather.9.cloned.1.call-start = ((), (), s32[]{:S(2)}) async-start(), calls=%async_computation.1 | async-start | bytes 5242880 | tf_op jit(solution)/shard_map/all_gather | solution.py:42
  7.3 81.3 %all-gather.13.cloned.1.call-start = ((), (), s32[]{:S(2)}) async-start(), calls=%async_computation.3 | async-start | bytes 1179648 | tf_op jit(solution)/shard_map/all_gather | solution.py:48
  8.0 121.7 %all-gather.15.cloned.1.call-start = ((), (), s32[]{:S(2)}) async-start(), calls=%async_computation.4 | async-start | bytes 1179648 | tf_op jit(solution)/shard_map/all_gather | solution.py:49
  8.7 162.0 %all-gather.11.cloned.1.call-start = ((), (), s32[]{:S(2)}) async-start(), calls=%async_computation.2 | async-start | bytes 1179648 | tf_op jit(solution)/shard_map/all_gather | solution.py:47
  9.3 201.4 %all-gather.17.cloned.1.call-start = ((), (), s32[]{:S(2)}) async-start(), calls=%async_computation.5 | async-start | bytes 1179648 | tf_op jit(solution)/shard_map/all_gather | solution.py:68
  9.9 290.1 %all-reduce.3.cloned.1.call-start = ((), (), s32[]{:S(2)}) async-start(), calls=%async_computation.6 | async-start | bytes 8388608 | tf_op jit(solution)/shard_map/psum | solution.py:71
  215.3 87.9 %copy-start.1 = (f32[2048]{0:T(1024)S(1)}, f32[2048]{0:T(1024)}, u32[]{:S(2)}) copy-start(f32[2048]{0:T(1024)} %param.20) | copy-start | bytes 24580
  215.3 179.3 %all-gather.19.cloned.1.call-start = ((), (), s32[]{:S(2)}) async-start(), calls=%async_computation.7 | async-start | bytes 6488064 | tf_op jit(solution)/shard_map/all_gather | solution.py:79
  216.1 271.3 %all-gather.21.cloned.1.call-start = ((), (), s32[]{:S(2)}) async-start(), calls=%async_computation.8 | async-start | bytes 6488064 | tf_op jit(solution)/shard_map/all_gather | solution.py:80
  216.8 363.9 %all-gather.23.cloned.1.call-start = ((), (), s32[]{:S(2)}) async-start(), calls=%async_computation.9 | async-start | bytes 6488064 | tf_op jit(solution)/shard_map/all_gather | solution.py:87
  217.5 426.8 %reduce-scatter.2.cloned.1.call-start = ((), (), s32[]{:S(2)}) async-start(), calls=%async_computation.10 | async-start | bytes 5242880 | tf_op jit(solution)/shard_map/reduce_scatter | solution.py:90
  300.0 3.4 copy-start
  303.4 91.2 %copy-start.3 = (f32[2048]{0:T(1024)S(1)}, f32[2048]{0:T(1024)}, u32[]{:S(2)}) copy-start(f32[2048]{0:T(1024)} %param.21) | copy-start | bytes 24580
Sparse Core Ops, SparseCore 0:
  8.9 37.1 all-gather.8
  48.2 40.2 all-gather.12
  90.7 38.9 all-gather.14
  131.7 38.9 all-gather.10
  172.6 38.0 all-gather.16
  215.4 84.4 all-reduce.2
  302.1 92.4 all-gather.18
  396.8 90.4 all-gather.20
  489.4 91.2 all-gather.22
  601.7 42.5 reduce-scatter.1
where the time goes:
time: 662 us; the launch traced here: 661 us
  waiting for transfers between devices  574 us (87%)
  matrix products  49.7 us (8%)
  other arithmetic  16.9 us (3%)
  between operations  13.6 us (2%)
    all_gather x1, waiting for transfers between devices, shards(): lax.all_gather(down_weight, 'fs', axis=1, tiled=True)  93.4 us
    all_gather x1, waiting for transfers between devices, shards(): lax.all_gather(gate_weight, 'fs', axis=0, tiled=True)  85.9 us
    psum x1, waiting for transfers between devices, shards(): merged = lax.psum(rounded_term(merged_part).astype(jnp.bfloat16), 'tp')  82.2 us
    all_gather x1, waiting for transfers between devices, shards(): lax.all_gather(up_weight, 'fs', axis=0, tiled=True)  80.7 us
    reduce_scatter x1, waiting for transfers between devices, shards(): lax.psum_scatter(rounded_term(down_part).astype(jnp.bfloat16), 'tp', scat...  42 us
    all_gather x1, waiting for transfers between devices, shards(): lax.all_gather(inner_weight, 'fs', axis=0, tiled=True)  39.4 us
    all_gather x1, waiting for transfers between devices, shards(): lax.all_gather(value_weight, 'fs', axis=0, tiled=True)  37.2 us
    all_gather x1, waiting for transfers between devices, shards(): lax.all_gather(outer_weight, 'fs', axis=0, tiled=True)  37 us
  transfers between devices with their start and end apart: 10, of which 10 were waited for; matrix products, arithmetic and copies ran while one was open for 6% of the time, Pallas kernels for 0%

commit v1 on v0

--- a/solution.py
+++ b/solution.py
@@ -39,7 +39,12 @@
     down_weight,
     output_gain,
 ):
-    whole_tokens = lax.all_gather(tokens, "tp", axis=1, tiled=True)
+    ring = [tokens]
+    for hop in range(3):
+        ring.append(lax.ppermute(ring[-1], "tp", [(dev, (dev + 1) % 4) for dev in range(4)]))
+    whole_tokens = jnp.roll(
+        jnp.concatenate(ring[::-1], axis=1), (lax.axis_index("tp") + 1) * ring[0].shape[1], axis=1
+    )
     normed = (normalize(whole_tokens) * mixer_gain).astype(jnp.bfloat16)
     length = normed.shape[0]
     channels = outer_weight.shape[1]

time: 662 us -> 626 us (0.946)
  waiting for transfers between devices: 574 us -> 531 us
  local copies, waits for them, and re-layouts: 0.99 us -> 8.9 us
    ppermute x0 -> x3, waiting for transfers between devices: none -> 42.1 us  [shards(): lax.ppermute(ring[-1], 'tp', [(dev, (dev + 1) % 4) for dev in range(4)])]
    all_gather x1, waiting for transfers between devices: 37.2 us -> 0.02 us  [shards(): lax.all_gather(value_weight, 'fs', axis=0, tiled=True)]
    all_gather x1 -> x0, waiting for transfers between devices: 35.5 us -> none  [shards(): whole_tokens = lax.all_gather(tokens, 'tp', axis=1, tiled=True)]
    all_gather x1, waiting for transfers between devices: 39.4 us -> 28.6 us  [shards(): lax.all_gather(inner_weight, 'fs', axis=0, tiled=True)]
    unnamed x8 -> x17, local copies, waits for them, and re-layouts: 0.21 us -> 7.98 us
  transfers between devices with their start and end apart: 10 -> 12, of which waited for: 10 -> 11; matrix products, arithmetic and copies ran while one was open for 6% -> 7% of each run, Pallas kernels for 0% -> 0%
where the time goes in v1:
time: 626 us; the launch traced here: 625 us
  waiting for transfers between devices  531 us (85%)
  matrix products  49.8 us (8%)
  other arithmetic  15.3 us (2%)
  between operations  13.4 us (2%)
  local copies, waits for them, and re-layouts  8.9 us (1%)
    all_gather x1, waiting for transfers between devices, shards(): lax.all_gather(down_weight, 'fs', axis=1, tiled=True)  93.4 us
    all_gather x1, waiting for transfers between devices, shards(): lax.all_gather(gate_weight, 'fs', axis=0, tiled=True)  85.4 us
    psum x1, waiting for transfers between devices, shards(): merged = lax.psum(rounded_term(merged_part).astype(jnp.bfloat16), 'tp')  82.3 us
    all_gather x1, waiting for transfers between devices, shards(): lax.all_gather(up_weight, 'fs', axis=0, tiled=True)  80.7 us
    ppermute x3, waiting for transfers between devices, shards(): lax.ppermute(ring[-1], 'tp', [(dev, (dev + 1) % 4) for dev in range(4)])  42.1 us
    reduce_scatter x1, waiting for transfers between devices, shards(): lax.psum_scatter(rounded_term(down_part).astype(jnp.bfloat16), 'tp', scat...  42 us
    all_gather x1, waiting for transfers between devices, shards(): lax.all_gather(outer_weight, 'fs', axis=0, tiled=True)  37.1 us
    all_gather x1, waiting for transfers between devices, shards(): lax.all_gather(merge_weight, 'fs', axis=1, tiled=True)  35.5 us
  transfers between devices with their start and end apart: 12, of which 11 were waited for; matrix products, arithmetic and copies ran while one was open for 7% of the time, Pallas kernels for 0%

profile of v1, /device:TPU:0, one launch (start us, length us, event | category | flops | bytes accessed | tf_op | source)
XLA Modules:
  0.0 625.1 jit_solution(16301622205248985992)
XLA Ops:
  8.8 14.4 %collective-permute-done = bf16[1024,512]{1,0:T(8,128)(2,1)S(1)} collective-permute-done((bf16[1024,512]{1,0:T(8,128)(2,1)}, bf16[1024,512]{1,0:T(8,128)(2,1)S(1)}, u32[]{:S(2)}, u32[]{:S(2)}) %collective-permute-start) | collective-permute-done | bytes 1048608 | tf_op jit(solution)/shard_map/ppermute | solution.py:44
  23.2 14.2 %collective-permute-done.1 = bf16[1024,512]{1,0:T(8,128)(2,1)S(1)} collective-permute-done((bf16[1024,512]{1,0:T(8,128)(2,1)S(1)}, bf16[1024,512]{1,0:T(8,128)(2,1)S(1)}, u32[]{:S(2)}, u32[]{:S(2)}) %collective-permute-start.1) | collective-permute-done | bytes 1048608 | tf_op jit(solution)/shard_map/ppermute | solution.py:44
  38.2 13.5 %collective-permute-done.2 = bf16[1024,512]{1,0:T(8,128)(2,1)} collective-permute-done((bf16[1024,512]{1,0:T(8,128)(2,1)S(1)}, bf16[1024,512]{1,0:T(8,128)(2,1)}, u32[]{:S(2)}, u32[]{:S(2)}) %collective-permute-start.2) | collective-permute-done | bytes 1048608 | tf_op jit(solution)/shard_map/ppermute | solution.py:44
  53.5 1.4 constant_dynamic-update-slice_fusion.4
  56.7 3.2 copy-done
  60.9 4.1 fusion.21
  65.0 28.6 %all-gather.10.cloned.1.call-done = bf16[2048,256]{1,0:T(8,128)(2,1)} async-done(((bf16[256,256]{1,0:T(8,128)(2,1)}), bf16[2048,256]{1,0:T(8,128)(2,1)}) %all-gather.10.cloned.1.call-update) | async-done | bytes 1048592 | tf_op jit(solution)/shard_map/all_gather | solution.py:53
  93.6 4.0 convolution_multiply_fusion
  97.6 37.1 %all-gather.8.cloned.1.call-done = bf16[2048,256]{1,0:T(8,128)(2,1)} async-done(((bf16[256,256]{1,0:T(8,128)(2,1)}), bf16[2048,256]{1,0:T(8,128)(2,1)}) %all-gather.8.cloned.1.call-update) | async-done | bytes 1048592 | tf_op jit(solution)/shard_map/all_gather | solution.py:52
  134.8 4.4 bitcast_reduce_fusion
  139.3 35.5 %all-gather.14.cloned.1.call-done = bf16[256,2048]{1,0:T(8,128)(2,1)} async-done(((bf16[256,256]{1,0:T(8,128)(2,1)}), bf16[256,2048]{1,0:T(8,128)(2,1)}) %all-gather.14.cloned.1.call-update) | async-done | bytes 1048592 | tf_op jit(solution)/shard_map/all_gather | solution.py:73
  174.8 4.6 convolution_convert_fusion.1
  181.7 82.3 %all-reduce.3.cloned.1.call-done = bf16[1024,2048]{1,0:T(8,128)(2,1)} async-done(((bf16[1024,2048]{1,0:T(8,128)(2,1)}), bf16[1024,2048]{1,0:T(8,128)(2,1)}) %all-reduce.3.cloned.1.call-update) | async-done | bytes 4194320 | tf_op jit(solution)/shard_map/psum | solution.py:76
  264.0 3.1 fusion
  267.1 6.0 fusion.2
  273.2 85.4 %all-gather.16.cloned.1.call-done = bf16[2048,1408]{1,0:T(8,128)(2,1)} async-done(((bf16[256,1408]{1,0:T(8,128)(2,1)}), bf16[2048,1408]{1,0:T(8,128)(2,1)}) %all-gather.16.cloned.1.call-update) | async-done | bytes 5767184 | tf_op jit(solution)/shard_map/all_gather | solution.py:84
  358.6 12.0 %fusion.14 = f32[1024,1408]{1,0:T(8,128)} fusion(bf16[2048,1408]{1,0:T(8,128)(2,1)} %all-gather.16.cloned.1.call-done, bf16[1024,2048]{1,0:T(8,128)(2,1)} %get-tuple-element.6, f32[2048]{0:T(1024)S(1)} %copy-done.4, f32[1024]{0:T(1024)S(1)} %add_rsqrt_fusion.2), kind=kOutput, calls=%fused_computation.27 | convolution fusion | flops 5913968640 | bytes 15740928 | tf_op jit(solution)/shard_map/dot_general | solution.py:87
  370.5 80.7 %all-gather.18.cloned.1.call-done = bf16[2048,1408]{1,0:T(8,128)(2,1)} async-done(((bf16[256,1408]{1,0:T(8,128)(2,1)}), bf16[2048,1408]{1,0:T(8,128)(2,1)}) %all-gather.18.cloned.1.call-update) | async-done | bytes 5767184 | tf_op jit(solution)/shard_map/all_gather | solution.py:85
  451.3 93.4 %all-gather.20.cloned.1.call-done = bf16[1408,2048]{1,0:T(8,128)(2,1)} async-done(((bf16[1408,256]{1,0:T(8,128)(2,1)}), bf16[1408,2048]{1,0:T(8,128)(2,1)}) %all-gather.20.cloned.1.call-update) | async-done | bytes 5767184 | tf_op jit(solution)/shard_map/all_gather | solution.py:92
  544.7 20.9 %convolution_convert_fusion = bf16[1024,2048]{1,0:T(8,128)(2,1)} fusion(bf16[1408,2048]{1,0:T(8,128)(2,1)} %all-gather.20.cloned.1.call-done, f32[1024,1408]{1,0:T(8,128)} %fusion.14, bf16[2048,1408]{1,0:T(8,128)(2,1)} %all-gather.18.cloned.1.call-done, bf16[1024,2048]{1,0:T(8,128)(2,1)} %get-tuple-element.6, f32[2048]{0:T(1024)S(1)} %copy-done.4, ...), kind=kOutput, calls=%fused_computation.17 | convolution fusion | flops 11830296576 | bytes 25702400 | tf_op jit(solution)/shard_map/dot_general | solution.py:90
  566.3 42.0 %reduce-scatter.2.cloned.1.call-done = bf16[1024,512]{1,0:T(8,128)(2,1)} async-done(((bf16[1024,2048]{1,0:T(8,128)(2,1)}), bf16[1024,512]{1,0:T(8,128)(2,1)}) %reduce-scatter.2.cloned.1.call-update) | async-done | bytes 1048592 | tf_op jit(solution)/shard_map/reduce_scatter | solution.py:95
  608.3 1.5 fusion.9
  609.8 5.8 psum.15
  615.6 3.0 fusion.12
  (48 shorter events, 10.6 us)
Async XLA Ops:
  6.5 50.0 %copy-start.1 = (bf16[1024,512]{1,0:T(8,128)(2,1)S(1)}, bf16[1024,512]{1,0:T(8,128)(2,1)}, u32[]{:S(2)}) copy-start(bf16[1024,512]{1,0:T(8,128)(2,1)} %param.13) | copy-start | bytes 3145732
  6.5 54.3 %all-gather.12.cloned.1.call-start = ((), (), s32[]{:S(2)}) async-start(), calls=%async_computation.3 | async-start | bytes 1179648 | tf_op jit(solution)/shard_map/all_gather | solution.py:54
  7.3 86.4 %all-gather.10.cloned.1.call-start = ((), (), s32[]{:S(2)}) async-start(), calls=%async_computation.2 | async-start | bytes 1179648 | tf_op jit(solution)/shard_map/all_gather | solution.py:53
  8.0 126.8 %all-gather.8.cloned.1.call-start = ((), (), s32[]{:S(2)}) async-start(), calls=%async_computation.1 | async-start | bytes 1179648 | tf_op jit(solution)/shard_map/all_gather | solution.py:52
  8.1 15.2 %collective-permute-start = (bf16[1024,512]{1,0:T(8,128)(2,1)}, bf16[1024,512]{1,0:T(8,128)(2,1)S(1)}, u32[]{:S(2)}, u32[]{:S(2)}) collective-permute-start(bf16[1024,512]{1,0:T(8,128)(2,1)} %param.13), channel_id=1, source_target_pairs={{0,1},{1,2},{2,3},{3,0},{4,5},{5,6},{6,7},{7,4},{8,9},{9,10},{10,1... | collective-permute-start | bytes 3145736 | tf_op jit(solution)/shard_map/ppermute | solution.py:44
  8.7 166.1 %all-gather.14.cloned.1.call-start = ((), (), s32[]{:S(2)}) async-start(), calls=%async_computation.4 | async-start | bytes 1179648 | tf_op jit(solution)/shard_map/all_gather | solution.py:73
  23.2 14.2 %collective-permute-start.1 = (bf16[1024,512]{1,0:T(8,128)(2,1)S(1)}, bf16[1024,512]{1,0:T(8,128)(2,1)S(1)}, u32[]{:S(2)}, u32[]{:S(2)}) collective-permute-start(bf16[1024,512]{1,0:T(8,128)(2,1)S(1)} %collective-permute-done), channel_id=1, source_target_pairs={{0,1},{1,2},{2,3},{3,0},{4,5},{5,6},{6,7},{7,4},{8,9},{9,10},{10,1... | collective-permute-start | bytes 3145736 | tf_op jit(solution)/shard_map/ppermute | solution.py:44
  37.4 14.3 %collective-permute-start.2 = (bf16[1024,512]{1,0:T(8,128)(2,1)S(1)}, bf16[1024,512]{1,0:T(8,128)(2,1)}, u32[]{:S(2)}, u32[]{:S(2)}) collective-permute-start(bf16[1024,512]{1,0:T(8,128)(2,1)S(1)} %collective-permute-done.1), channel_id=1, source_target_pairs={{0,1},{1,2},{2,3},{3,0},{4,5},{5,6},{6,7},{7,4},{8,9},{9,10},{10,1... | collective-permute-start | bytes 3145736 | tf_op jit(solution)/shard_map/ppermute | solution.py:44
  37.5 226.6 %all-reduce.3.cloned.1.call-start = ((), (), s32[]{:S(2)}) async-start(), calls=%async_computation.5 | async-start | bytes 8388608 | tf_op jit(solution)/shard_map/psum | solution.py:76
  53.3 7.6 %copy-start.3 = (f32[2048]{0:T(1024)S(1)}, f32[2048]{0:T(1024)}, u32[]{:S(2)}) copy-start(f32[2048]{0:T(1024)} %param.14) | copy-start | bytes 24580
  56.7 3.2 copy-start
  139.2 127.9 %copy-start.2 = (f32[2048]{0:T(1024)S(1)}, f32[2048]{0:T(1024)}, u32[]{:S(2)}) copy-start(f32[2048]{0:T(1024)} %param.20) | copy-start | bytes 24580
  179.4 179.2 %all-gather.16.cloned.1.call-start = ((), (), s32[]{:S(2)}) async-start(), calls=%async_computation.6 | async-start | bytes 6488064 | tf_op jit(solution)/shard_map/all_gather | solution.py:84
  180.0 271.3 %all-gather.18.cloned.1.call-start = ((), (), s32[]{:S(2)}) async-start(), calls=%async_computation.7 | async-start | bytes 6488064 | tf_op jit(solution)/shard_map/all_gather | solution.py:85
  180.7 363.9 %all-gather.20.cloned.1.call-start = ((), (), s32[]{:S(2)}) async-start(), calls=%async_computation.8 | async-start | bytes 6488064 | tf_op jit(solution)/shard_map/all_gather | solution.py:92
  181.5 177.1 %copy-start.4 = (f32[2048]{0:T(1024)S(1)}, f32[2048]{0:T(1024)}, u32[]{:S(2)}) copy-start(f32[2048]{0:T(1024)} %param.21) | copy-start | bytes 24580
  181.5 426.8 %reduce-scatter.2.cloned.1.call-start = ((), (), s32[]{:S(2)}) async-start(), calls=%async_computation.9 | async-start | bytes 5242880 | tf_op jit(solution)/shard_map/reduce_scatter | solution.py:95
Sparse Core Ops, SparseCore 0:
  9.5 42.9 all-gather.11
  54.6 38.9 all-gather.9
  95.7 38.9 all-gather.7
  136.7 38.0 all-gather.13
  179.5 84.4 all-reduce.2
  266.1 92.4 all-gather.15
  360.8 90.4 all-gather.17
  453.3 91.2 all-gather.19
  565.7 42.5 reduce-scatter.1
